TPU v7x, 32 devices: a whole 2x2x4 slice. The times are simulated.
32 devices in a mesh: kv: 8 (over z, y), tp: 4 (over x, core).
Axes of the slice: x: 2, y: 2, z: 4, core: 2. Of those that a mesh axis runs over, the one named last changes fastest.
Arguments:
- tokens: bfloat16 [32, 4096], P(None, 'kv'), may hold values from -8 to 8, as said below
- attn_gain: float32 [4096], P('kv'), may hold values from 0.1 to 1.9
- query_weight: bfloat16 [4096, 1024], P('kv', 'tp'), may hold values from -0.09375 to 0.09375
- key_weight: bfloat16 [4096, 1024], P('kv', 'tp'), may hold values from -0.09375 to 0.09375
- value_weight: bfloat16 [4096, 2048], P('kv', 'tp'), may hold values from -0.09375 to 0.09375
- outgate_weight: bfloat16 [4096, 2048], P('kv', 'tp'), may hold values from -0.09375 to 0.09375
- code_weight: bfloat16 [4096, 16], P('kv'), may hold values from -0.09375 to 0.09375
- decay_weight: bfloat16 [16, 1024], P(None, 'tp'), may hold values from -6 to 6
- decay_bias: float32 [1024], P('tp'), may hold values from -4 to 2
- head_gain: float32 [256], replicated, may hold values from 0.1 to 1.9
- key_cache: bfloat16 [32, 64, 8, 128], P('kv', None, 'tp'), may hold values from -6 to 6
- value_cache: bfloat16 [32, 64, 8, 256], P('kv', None, 'tp'), may hold values from -6 to 6
- decay_cache: float32 [32, 64, 8, 128], P('kv', None, 'tp'), may hold values from -1.1 to 0
- carried_state: float32 [32, 8, 128, 256], P('kv', 'tp'), may hold values from -24 to 24
- lengths: int32 [32], P('kv'), may hold values from 1 to 64, 832 in all
- output_weight: bfloat16 [2048, 4096], P('tp', 'kv'), may hold values from -0.125 to 0.125
- mlp_gain: float32 [4096], P('kv'), may hold values from 0.1 to 1.9
- gate_weight: bfloat16 [4096, 11008], P('kv', 'tp'), may hold values from -0.09375 to 0.09375
- up_weight: bfloat16 [4096, 11008], P('kv', 'tp'), may hold values from -0.09375 to 0.09375
- down_weight: bfloat16 [11008, 4096], P('tp', 'kv'), may hold values from -0.0546875 to 0.0546875
Outputs:
- layer_out: bfloat16 [32, 4096], P(None, 'kv')
- new_keys: bfloat16 [32, 8, 128], P('kv', 'tp')
- new_values: bfloat16 [32, 8, 256], P('kv', 'tp')
Inputs may be any that keep to these rules, and one draw needn't show every extreme that they name: `tokens`: the features of a row have unlike scales. Sequence b's new token comes right after its lengths[b] live positions; positions from lengths[b] on take no part.
All inputs are finite; a program needn't handle non-finite values. No bound on the sum of `lengths` on one device may be relied on, other than what follows from the above.
Results may differ from a plain program's by a relative error of at most 0.025.
Values may be sent and summed in bfloat16 or wider, within the bound.
A program may use at most 64 MiB of HBM per device.

v0:
```python
import functools

import jax
import jax.numpy as jnp
from jax import lax
from jax.experimental import pallas as pl
from jax.experimental.pallas import tpu as pltpu
from jax.sharding import PartitionSpec as P

EPS = 1e-06
GATE_TEMP = 16.0
FIRST_LOADS = 7
PARTS = 4
LANES = 128
F32 = jnp.float32
BF16 = jnp.bfloat16


def split_sum(column):
    high = column.astype(BF16).astype(F32)
    return high, column - high


def dot(left, right):
    return jnp.dot(left, right, preferred_element_type=F32)


def dot_t(left, right):
    return lax.dot_general(left, right, (((1,), (1,)), ((), ())), preferred_element_type=F32)


def tiles_of(total, step):
    return [(start, min(step, total - start)) for start in range(0, total, step)]


def pieces_of(units):
    each = units // PARTS // LANES * LANES
    head = units - (PARTS - 1) * each
    room = (head + 2 + LANES - 1) // LANES * LANES
    return [(0, head, room)] + [(head + k * each, each, each) for k in range(PARTS - 1)]


def copy_out(*refs):
    *arrays, sems = refs
    half = len(arrays) // 2
    copies = [
        pltpu.make_async_copy(arrays[k], arrays[half + k], sems.at[k]) for k in range(half)
    ]
    for copy in copies:
        copy.start()
    for copy in copies:
        copy.wait()


def layer_kernel(
    n_kv,
    n_tp,
    width,
    tokens_h,
    attn_gain_h,
    wq_h,
    wk_h,
    wv_h,
    wg_h,
    wc_h,
    dw_h,
    db_h,
    head_gain_h,
    key_h,
    value_h,
    decay_h,
    state_h,
    lengths_s,
    wo_h,
    mlp_gain_h,
    gate_h,
    up_h,
    down_h,
    out_ref,
    nk_ref,
    nv_ref,
    tokens,
    attn_gain,
    wq,
    wk,
    wv,
    wg,
    wc,
    dw,
    db,
    head_gain,
    key,
    value,
    decay,
    state,
    wo,
    mlp_gain,
    gate,
    up,
    down,
    proj,
    proj_send,
    proj_recv,
    keyed,
    total_exp,
    decayed3,
    keys3,
    values3,
    mixed,
    heads,
    heads_all,
    attended,
    accs,
    sends,
    recvs,
    hiddens,
    hiddens_all,
    lifted,
    load_sem,
    send_a,
    recv_a,
    send_b,
    recv_b,
    send_c,
    recv_c,
    send_d,
    recv_d,
    send_e,
    recv_e,
    send_f,
    recv_f,
):
    kv_me = lax.axis_index("kv")
    tp_me = lax.axis_index("tp")
    rows, feats = tokens.shape
    seqs, span, heads_here, key_dim = key.shape
    value_dim = value.shape[3]
    kw, vw = heads_here * key_dim, heads_here * value_dim
    rank = wc.shape[0]
    units = gate.shape[0]
    pieces = pieces_of(units)

    loads = {}
    pairs = [
        ("tokens", tokens_h, tokens),
        ("attn_gain", attn_gain_h, attn_gain),
        ("wc", wc_h, wc),
        ("wq", wq_h, wq),
        ("wk", wk_h, wk),
        ("wv", wv_h, wv),
        ("wg", wg_h, wg),
        ("decay", decay_h, decay),
        ("key", key_h, key),
        ("dw", dw_h, dw.at[pl.ds(0, rank)]),
        ("db", db_h, db),
        ("head_gain", head_gain_h, head_gain),
        ("state", state_h, state),
        ("value", value_h, value),
        ("wo", wo_h, wo),
        ("mlp_gain", mlp_gain_h, mlp_gain),
        ("gate", gate_h, gate),
        ("up", up_h, up),
        ("down", down_h, down),
    ]
    for place, (name, source, target) in enumerate(pairs):
        loads[name] = pltpu.make_async_copy(source, target, load_sem.at[place])
        if place < FIRST_LOADS:
            loads[name].start()

    def ready(*names):
        for name in names:
            loads.pop(name).wait()

    barrier = pltpu.get_barrier_semaphore()
    for off in range(1, n_kv):
        pl.semaphore_signal(
            barrier,
            inc=1,
            device_id={"kv": lax.rem(kv_me + off, n_kv)},
            device_id_type=pl.DeviceIdType.MESH,
        )
    for off in range(1, n_tp):
        pl.semaphore_signal(
            barrier,
            inc=1,
            device_id={"tp": lax.rem(tp_me + off, n_tp)},
            device_id_type=pl.DeviceIdType.MESH,
        )

    def exchange(axis, me, count, source, target, sent, arrived):
        started = []
        for off in range(count - 1, 0, -1):
            p = lax.rem(me + off, count)
            copy = pltpu.make_async_remote_copy(
                src_ref=source(p),
                dst_ref=target.at[me],
                send_sem=sent.at[off],
                recv_sem=arrived.at[me],
                device_id={axis: p},
                device_id_type=pl.DeviceIdType.MESH,
            )
            copy.start()
            started.append(copy)
        return started

    def await_arrivals(me, count, target, arrived):
        for off in range(1, count):
            p = lax.rem(me + off, count)
            pltpu.make_async_copy(target.at[p], target.at[p], arrived.at[p]).wait()

    pending = []

    base_misc = 2 * kw + 2 * vw
    ready(*("tokens", "attn_gain", "wc"))
    token_f = tokens[...].astype(F32)
    scaled = (token_f * attn_gain[...]).astype(BF16)
    proj[:, base_misc:] = jnp.zeros((rows, LANES), F32)
    proj[:, base_misc : base_misc + rank] = dot_t(scaled, wc[...])
    high, low = split_sum(jnp.sum(token_f * token_f, axis=1, keepdims=True))
    proj[:, base_misc + rank : base_misc + rank + 1] = high
    proj[:, base_misc + rank + 1 : base_misc + rank + 2] = low
    base = 0
    for name, weight in (("wq", wq), ("wk", wk), ("wv", wv), ("wg", wg)):
        ready(name)
        if name == "wg":
            for late in list(loads.values()):
                late.start()
        for start, size in tiles_of(weight.shape[1], 256):
            proj[:, base + start : base + start + size] = dot(
                scaled, weight[:, start : start + size]
            )
        base += weight.shape[1]
    for p in range(n_kv):
        proj_send[p] = proj[p * seqs : (p + 1) * seqs, :].astype(BF16)
    pl.semaphore_wait(barrier, n_kv + n_tp - 2)
    pending += exchange("kv", kv_me, n_kv, lambda p: proj_send.at[p], proj_recv, send_a, recv_a)
    proj_recv[kv_me] = proj_send[kv_me]

    dw[rank:, :] = jnp.zeros((dw.shape[0] - rank, dw.shape[1]), BF16)
    ready("decay")
    ready("key")
    positions = lax.broadcasted_iota(jnp.int32, (span, heads_here, key_dim), 0)
    for b in range(seqs):
        live = positions < lengths_s[b]
        kept = jnp.where(live, decay[b], 0.0)
        suffix = kept
        step = 1
        while step < span:
            suffix = suffix + jnp.concatenate(
                [suffix[step:], jnp.zeros((step, heads_here, key_dim), F32)], axis=0
            )
            step *= 2
        total_exp[b] = jnp.exp(suffix[0])
        later = jnp.concatenate([suffix[1:], jnp.zeros((1, heads_here, key_dim), F32)], axis=0)
        keyed[b] = jnp.where(live, key[b].astype(F32) * jnp.exp(later), 0.0)
    ready(*("dw", "db", "head_gain", "state", "value"))

    await_arrivals(kv_me, n_kv, proj_recv, recv_a)
    total = proj_recv[0].astype(F32)
    for p in range(1, n_kv):
        total = total + proj_recv[p].astype(F32)
    misc = total[:, base_misc:]
    squares = misc[:, rank : rank + 1] + misc[:, rank + 1 : rank + 2]
    inv_rms = lax.rsqrt(squares / width + EPS)
    queries = (total[:, :kw] * inv_rms * key_dim ** (-0.5)).astype(BF16).astype(F32)
    new_keys = (total[:, kw : 2 * kw] * inv_rms).astype(BF16).astype(F32)
    new_values = (total[:, 2 * kw : 2 * kw + vw] * inv_rms).astype(BF16).astype(F32)
    out_gate = (total[:, 2 * kw + vw : base_misc] * inv_rms).astype(BF16).astype(F32)
    code = (misc * inv_rms).astype(BF16)
    pre_gate = dot(code, dw[...]) + db[...]
    new_decay = (jnp.minimum(pre_gate, 0.0) - jnp.log1p(jnp.exp(-jnp.abs(pre_gate)))) / GATE_TEMP
    decayed = queries * jnp.exp(new_decay)
    for b in range(seqs):
        for h in range(heads_here):
            k_cols = slice(h * key_dim, (h + 1) * key_dim)
            v_cols = slice(h * value_dim, (h + 1) * value_dim)
            decayed3[b, h : h + 1, :] = decayed[b : b + 1, k_cols]
            keys3[b, h : h + 1, :] = new_keys[b : b + 1, k_cols]
            values3[b, h : h + 1, :] = new_values[b : b + 1, v_cols]
    nk_ref[...] = keys3[...].astype(BF16)
    nv_ref[...] = values3[...].astype(BF16)
    for b in range(seqs):
        d = decayed3[b]
        scores = jnp.sum(keyed[b] * d[None], axis=-1, keepdims=True)
        scores = scores.astype(BF16).astype(F32)
        within = jnp.sum(scores * value[b].astype(F32), axis=0)
        into_state = jnp.transpose(
            jnp.concatenate(
                [d * total_exp[b], jnp.zeros((8 - heads_here, key_dim), F32)], axis=0
            )
        )
        for h in range(heads_here):
            carried = jnp.sum(into_state[:, h : h + 1] * state[b, h], axis=0, keepdims=True)
            mixed[b : b + 1, h * value_dim : (h + 1) * value_dim] = carried + within[h : h + 1]
    for h in range(heads_here):
        k_cols = slice(h * key_dim, (h + 1) * key_dim)
        v_cols = slice(h * value_dim, (h + 1) * value_dim)
        own = jnp.sum(queries[:, k_cols] * new_keys[:, k_cols], axis=-1, keepdims=True)
        full = mixed[:, v_cols] + own * new_values[:, v_cols]
        norm = lax.rsqrt(jnp.mean(full * full, axis=-1, keepdims=True) + EPS)
        g = out_gate[:, v_cols]
        mixed[:, v_cols] = full * norm * head_gain[...] * (g / (1.0 + jnp.exp(-g)))
    heads_all[kv_me] = mixed[...].astype(BF16)
    pending += exchange(
        "kv", kv_me, n_kv, lambda p: heads_all.at[kv_me], heads_all, send_b, recv_b
    )

    ready("wo")
    ready("mlp_gain")
    await_arrivals(kv_me, n_kv, heads_all, recv_b)
    for p in range(n_kv):
        heads[p * seqs : (p + 1) * seqs, :] = heads_all[p].astype(F32)
    attended[tp_me] = dot(heads[...].astype(BF16), wo[...]).astype(BF16)
    pending += exchange(
        "tp", tp_me, n_tp, lambda p: attended.at[tp_me], attended, send_c, recv_c
    )
    ready("gate")
    await_arrivals(tp_me, n_tp, attended, recv_c)
    summed = attended[0].astype(F32)
    for p in range(1, n_tp):
        summed = summed + attended[p].astype(F32)
    mid_f = (token_f + summed).astype(BF16).astype(F32)
    scaled_mid = (mid_f * mlp_gain[...]).astype(BF16)

    ready("up")
    for part, (first, size, span_cols) in enumerate(pieces):
        mlp_acc = accs[part]
        for base, weight in ((0, gate), (span_cols, up)):
            if size < span_cols:
                mlp_acc[:, base + span_cols - LANES : base + span_cols] = jnp.zeros(
                    (rows, LANES), F32
                )
            for start, count in tiles_of(size, 256):
                mlp_acc[:, base + start : base + start + count] = dot_t(
                    scaled_mid, weight[first + start : first + start + count, :]
                )
        if part == 0:
            high, low = split_sum(jnp.sum(mid_f * mid_f, axis=1, keepdims=True))
            mlp_acc[:, size : size + 1] = high
            mlp_acc[:, size + 1 : size + 2] = low
        for p in range(n_kv):
            sends[part][p] = mlp_acc[p * seqs : (p + 1) * seqs, :].astype(BF16)
        pending += exchange(
            "kv",
            kv_me,
            n_kv,
            lambda p, part=part: sends[part].at[p],
            recvs[part],
            send_d.at[part],
            recv_d.at[part],
        )
        recvs[part][kv_me] = sends[part][kv_me]
    for part, (first, size, span_cols) in enumerate(pieces):
        await_arrivals(kv_me, n_kv, recvs[part], recv_d.at[part])
        total = recvs[part][0].astype(F32)
        for p in range(1, n_kv):
            total = total + recvs[part][p].astype(F32)
        if part == 0:
            squares = total[:, size : size + 1] + total[:, size + 1 : size + 2]
            inv_mid = lax.rsqrt(squares / width + EPS)
        g = total[:, :span_cols] * inv_mid
        mine = g / (1.0 + jnp.exp(-g)) * (total[:, span_cols:] * inv_mid)
        hiddens_all[part][kv_me] = mine.astype(BF16)
        pending += exchange(
            "kv",
            kv_me,
            n_kv,
            lambda p, part=part: hiddens_all[part].at[kv_me],
            hiddens_all[part],
            send_e.at[part],
            recv_e.at[part],
        )
    ready("down")
    acc = jnp.zeros((rows, feats), F32)
    for part, (first, size, span_cols) in enumerate(pieces):
        await_arrivals(kv_me, n_kv, hiddens_all[part], recv_e.at[part])
        hidden = hiddens[part]
        for p in range(n_kv):
            hidden[p * seqs : (p + 1) * seqs, :] = hiddens_all[part][p].astype(F32)
        if size < span_cols:
            lane = lax.broadcasted_iota(jnp.int32, (rows, span_cols), 1)
            whole = jnp.where(lane < size, hidden[...], 0.0).astype(BF16)
        else:
            whole = hidden[...].astype(BF16)
        acc = acc + dot(whole, down[first : first + span_cols, :])
    lifted[tp_me] = acc.astype(BF16)
    pending += exchange("tp", tp_me, n_tp, lambda p: lifted.at[tp_me], lifted, send_f, recv_f)
    await_arrivals(tp_me, n_tp, lifted, recv_f)
    summed = lifted[0].astype(F32)
    for p in range(1, n_tp):
        summed = summed + lifted[p].astype(F32)
    out_ref[...] = (mid_f + summed).astype(BF16)
    for copy in pending:
        copy.wait_send()


def on_device(n_kv, n_tp, *args):
    (
        tokens,
        attn_gain,
        wq,
        wk,
        wv,
        wg,
        wc,
        dw,
        db,
        head_gain,
        key,
        value,
        decay,
        state,
        lengths,
        wo,
        mlp_gain,
        gate,
        up,
        down,
    ) = args
    row = lambda a: a.reshape(1, a.shape[0])
    operands = [
        tokens,
        row(attn_gain),
        wq,
        wk,
        wv,
        wg,
        wc.T,
        dw,
        row(db),
        row(head_gain),
        key,
        value,
        decay,
        state,
        lengths,
        wo,
        row(mlp_gain),
        gate.T,
        up.T,
        down,
    ]
    rows, feats = tokens.shape
    seqs, span, heads_here, key_dim = key.shape
    value_dim = value.shape[3]
    kw, vw = heads_here * key_dim, heads_here * value_dim
    units = gate.shape[1]
    rank = wc.shape[1]
    widths = [piece[2] for piece in pieces_of(units)]
    cols = 2 * kw + 2 * vw + LANES
    vmem = pltpu.VMEM

    def copied(a):
        if a is lengths:
            return None
        if a is dw:
            return vmem((LANES, a.shape[1]), a.dtype)
        return vmem(a.shape, a.dtype)

    scratch = [c for c in map(copied, operands) if c is not None]
    scratch += [
        vmem((rows, cols), F32),
        vmem((n_kv, seqs, cols), BF16),
        vmem((n_kv, seqs, cols), BF16),
        vmem((seqs, span, heads_here, key_dim), F32),
        vmem((seqs, heads_here, key_dim), F32),
        vmem((seqs, heads_here, key_dim), F32),
        vmem((seqs, heads_here, key_dim), F32),
        vmem((seqs, heads_here, value_dim), F32),
        vmem((seqs, vw), F32),
        vmem((rows, vw), F32),
        vmem((n_kv, seqs, vw), BF16),
        vmem((n_tp, rows, feats), BF16),
        [vmem((rows, 2 * w), F32) for w in widths],
        [vmem((n_kv, seqs, 2 * w), BF16) for w in widths],
        [vmem((n_kv, seqs, 2 * w), BF16) for w in widths],
        [vmem((rows, w), F32) for w in widths],
        [vmem((n_kv, seqs, w), BF16) for w in widths],
        vmem((n_tp, rows, feats), BF16),
    ]
    dma = pltpu.SemaphoreType.DMA
    scratch += [dma((19,))]
    scratch += [dma((n_kv,))] * 4
    scratch += [dma((n_tp,))] * 2
    scratch += [dma((PARTS, n_kv))] * 4
    scratch += [dma((n_tp,))] * 2
    hbm_spec = pl.BlockSpec(memory_space=pltpu.HBM)
    in_specs = [
        pl.BlockSpec(memory_space=pltpu.SMEM) if a is lengths else hbm_spec for a in operands
    ]
    shapes = ((rows, feats), (seqs, heads_here, key_dim), (seqs, heads_here, value_dim))
    results = pl.pallas_call(
        functools.partial(layer_kernel, n_kv, n_tp, feats * n_kv),
        out_shape=tuple(vmem(shape, BF16) for shape in shapes),
        in_specs=in_specs,
        out_specs=(pl.BlockSpec(memory_space=pltpu.VMEM),) * 3,
        scratch_shapes=scratch,
        compiler_params=pltpu.CompilerParams(
            collective_id=0, has_side_effects=True, vmem_limit_bytes=66900000
        ),
        name="layer",
    )(*operands)
    local = (pl.BlockSpec(memory_space=pl.ANY),) * 3
    return pl.pallas_call(
        copy_out,
        out_shape=tuple(jax.ShapeDtypeStruct(shape, BF16) for shape in shapes),
        in_specs=local,
        out_specs=local,
        scratch_shapes=[dma((3,))],
        name="results",
    )(*results)


def solution(mesh):
    in_specs = (
        P(None, "kv"),
        P("kv"),
        P("kv", "tp"),
        P("kv", "tp"),
        P("kv", "tp"),
        P("kv", "tp"),
        P("kv", None),
        P(None, "tp"),
        P("tp"),
        P(),
        P("kv", None, "tp", None),
        P("kv", None, "tp", None),
        P("kv", None, "tp", None),
        P("kv", "tp", None, None),
        P("kv"),
        P("tp", "kv"),
        P("kv"),
        P("kv", "tp"),
        P("kv", "tp"),
        P("tp", "kv"),
    )
    out_specs = (P(None, "kv"), P("kv", "tp", None), P("kv", "tp", None))
    return jax.shard_map(
        functools.partial(on_device, mesh.shape["kv"], mesh.shape["tp"]),
        mesh=mesh,
        in_specs=in_specs,
        out_specs=out_specs,
        check_vma=False,
    )
```

profile of v0, /device:TPU:0, one launch (start us, length us, event | category | flops | bytes accessed | tf_op | source)
XLA Modules:
  0.0 45.2 jit_solution(14607715888663723003)
XLA Ops:
  0.6 40.4 %layer.1 = (bf16[32,512]{1,0:T(8,128)(2,1)S(1)}, bf16[4,2,128]{2,1,0:T(2,128)(2,1)S(1)}, bf16[4,2,256]{2,1,0:T(2,128)(2,1)S(1)}) custom-call(bf16[32,512]{1,0:T(8,128)(2,1)} %tokens_h.1, f32[1,512]{1,0:T(1,128)} %bitcast.10, bf16[512,256]{1,0:T(8,128)(2,1)} %wq_h.1, bf16[512,256]{1,0:T(8,128)(2,1)} %wk_h.1, bf16[512,512]{1,0:T(8,128)(2,1)} %wv_h.1, ...), custom_call_target="tpu_custom_call" | custom-call | tf_op jit(solution)/shard_map/layer/pallas_call | solution.py:492
  41.1 0.0 copy-start
  41.1 0.6 %copy-done = bf16[32,512]{1,0:T(8,128)(2,1)} copy-done((bf16[32,512]{1,0:T(8,128)(2,1)}, bf16[32,512]{1,0:T(8,128)(2,1)S(1)}, u32[]{:S(2)}) %copy-start) | copy-done | bytes 32792
  41.7 0.0 copy-start.2
  41.7 0.6 %copy-done.2 = bf16[4,2,128]{2,1,0:T(2,128)(2,1)} copy-done((bf16[4,2,128]{2,1,0:T(2,128)(2,1)}, bf16[4,2,128]{2,1,0:T(2,128)(2,1)S(1)}, u32[]{:S(2)}) %copy-start.2) | copy-done | bytes 2072
  42.3 0.0 copy-start.1
  42.3 0.6 %copy-done.1 = bf16[4,2,256]{2,1,0:T(2,128)(2,1)} copy-done((bf16[4,2,256]{2,1,0:T(2,128)(2,1)}, bf16[4,2,256]{2,1,0:T(2,128)(2,1)S(1)}, u32[]{:S(2)}) %copy-start.1) | copy-done | bytes 4120
  42.9 2.3 %results.1 = (bf16[32,512]{1,0:T(8,128)(2,1)}, bf16[4,2,128]{2,1,0:T(2,128)(2,1)}, bf16[4,2,256]{2,1,0:T(2,128)(2,1)}) custom-call(bf16[32,512]{1,0:T(8,128)(2,1)} %copy-done, bf16[4,2,128]{2,1,0:T(2,128)(2,1)} %copy-done.2, bf16[4,2,256]{2,1,0:T(2,128)(2,1)} %copy-done.1), custom_call_target="tpu_custom_call" | custom-call | tf_op jit(solution)/shard_map/results/pallas_call | solution.py:504
Async XLA Ops:
  41.1 0.6 %copy-start = (bf16[32,512]{1,0:T(8,128)(2,1)}, bf16[32,512]{1,0:T(8,128)(2,1)S(1)}, u32[]{:S(2)}) copy-start(bf16[32,512]{1,0:T(8,128)(2,1)S(1)} %get-tuple-element.6.refs_0_) | copy-start | bytes 98308
  41.7 0.6 %copy-start.2 = (bf16[4,2,128]{2,1,0:T(2,128)(2,1)}, bf16[4,2,128]{2,1,0:T(2,128)(2,1)S(1)}, u32[]{:S(2)}) copy-start(bf16[4,2,128]{2,1,0:T(2,128)(2,1)S(1)} %get-tuple-element.7.refs_1_) | copy-start | bytes 6148
  42.3 0.6 %copy-start.1 = (bf16[4,2,256]{2,1,0:T(2,128)(2,1)}, bf16[4,2,256]{2,1,0:T(2,128)(2,1)S(1)}, u32[]{:S(2)}) copy-start(bf16[4,2,256]{2,1,0:T(2,128)(2,1)S(1)} %get-tuple-element.8.refs_2_) | copy-start | bytes 12292
where the time goes:
time: 45.3 us; the launch traced here: 45.2 us
  Pallas kernels  42.7 us (94%)
  local copies, waits for them, and re-layouts  1.78 us (4%)
  between operations  0.66 us (1%)
    pallas_call x1, Pallas kernels, on_device(): pl.pallas_call(functools.partial(layer_kernel, n_kv, n_tp, feats * n_kv),...  40.4 us
    pallas_call x1, Pallas kernels, on_device(): pl.pallas_call(copy_out, out_shape=tuple((jax.ShapeDtypeStruct(shape, BF1...  2.3 us
    unnamed x6, local copies, waits for them, and re-layouts  1.78 us

commit v1 on v0

--- a/solution.py
+++ b/solution.py
@@ -11,6 +11,7 @@
 GATE_TEMP = 16.0
 FIRST_LOADS = 7
 PARTS = 4
+SHARED_SEMS = 5
 LANES = 128
 F32 = jnp.float32
 BF16 = jnp.bfloat16
@@ -38,6 +39,21 @@
     head = units - (PARTS - 1) * each
     room = (head + 2 + LANES - 1) // LANES * LANES
     return [(0, head, room)] + [(head + k * each, each, each) for k in range(PARTS - 1)]
+
+
+def peer_of(me, step, count):
+    if count & (count - 1):
+        return lax.rem(me + step, count)
+    place, bit = 0, 1
+    while bit < count:
+        own = lax.rem(me // bit, 2)
+        place = place + bit * (1 - own if step & bit else own)
+        bit *= 2
+    return place
+
+
+def drain(ref, sem):
+    pltpu.make_async_copy(ref, ref, sem).wait()
 
 
 def copy_out(*refs):
@@ -70,7 +86,7 @@
     value_h,
     decay_h,
     state_h,
-    lengths_s,
+    lengths_h,
     wo_h,
     mlp_gain_h,
     gate_h,
@@ -93,11 +109,15 @@
     value,
     decay,
     state,
+    lengths_s,
     wo,
     mlp_gain,
     gate,
     up,
     down,
+    early,
+    early_send,
+    early_recv,
     proj,
     proj_send,
     proj_recv,
@@ -117,18 +137,8 @@
     hiddens_all,
     lifted,
     load_sem,
-    send_a,
-    recv_a,
-    send_b,
-    recv_b,
-    send_c,
-    recv_c,
-    send_d,
-    recv_d,
-    send_e,
-    recv_e,
-    send_f,
-    recv_f,
+    send_sem,
+    recv_sem,
 ):
     kv_me = lax.axis_index("kv")
     tp_me = lax.axis_index("tp")
@@ -149,6 +159,7 @@
         ("wk", wk_h, wk),
         ("wv", wv_h, wv),
         ("wg", wg_h, wg),
+        ("lengths", lengths_h, lengths_s),
         ("decay", decay_h, decay),
         ("key", key_h, key),
         ("dw", dw_h, dw.at[pl.ds(0, rank)]),
@@ -187,58 +198,60 @@
             device_id_type=pl.DeviceIdType.MESH,
         )
 
-    def exchange(axis, me, count, source, target, sent, arrived):
-        started = []
-        for off in range(count - 1, 0, -1):
-            p = lax.rem(me + off, count)
-            copy = pltpu.make_async_remote_copy(
+    pending = []
+
+    def exchange(axis, me, count, source, target, sem):
+        for step in range(count - 1, 0, -1):
+            p = peer_of(me, step, count)
+            pltpu.make_async_remote_copy(
                 src_ref=source(p),
                 dst_ref=target.at[me],
-                send_sem=sent.at[off],
-                recv_sem=arrived.at[me],
+                send_sem=send_sem.at[sem],
+                recv_sem=recv_sem.at[sem],
                 device_id={axis: p},
                 device_id_type=pl.DeviceIdType.MESH,
-            )
-            copy.start()
-            started.append(copy)
-        return started
-
-    def await_arrivals(me, count, target, arrived):
-        for off in range(1, count):
-            p = lax.rem(me + off, count)
-            pltpu.make_async_copy(target.at[p], target.at[p], arrived.at[p]).wait()
-
-    pending = []
-
-    base_misc = 2 * kw + 2 * vw
+            ).start()
+        pending.append((target.at[pl.ds(0, count - 1)], sem))
+
+    def await_arrivals(count, target, sem):
+        drain(target.at[pl.ds(0, count - 1)], recv_sem.at[sem])
+
+    base_misc = 2 * kw
     ready(*("tokens", "attn_gain", "wc"))
     token_f = tokens[...].astype(F32)
     scaled = (token_f * attn_gain[...]).astype(BF16)
-    proj[:, base_misc:] = jnp.zeros((rows, LANES), F32)
-    proj[:, base_misc : base_misc + rank] = dot_t(scaled, wc[...])
+    early[:, base_misc:] = jnp.zeros((rows, LANES), F32)
+    early[:, base_misc : base_misc + rank] = dot_t(scaled, wc[...])
     high, low = split_sum(jnp.sum(token_f * token_f, axis=1, keepdims=True))
-    proj[:, base_misc + rank : base_misc + rank + 1] = high
-    proj[:, base_misc + rank + 1 : base_misc + rank + 2] = low
-    base = 0
-    for name, weight in (("wq", wq), ("wk", wk), ("wv", wv), ("wg", wg)):
+    early[:, base_misc + rank : base_misc + rank + 1] = high
+    early[:, base_misc + rank + 1 : base_misc + rank + 2] = low
+
+    def project(result, base, name, weight):
         ready(name)
         if name == "wg":
             for late in list(loads.values()):
                 late.start()
         for start, size in tiles_of(weight.shape[1], 256):
-            proj[:, base + start : base + start + size] = dot(
+            result[:, base + start : base + start + size] = dot(
                 scaled, weight[:, start : start + size]
             )
-        base += weight.shape[1]
-    for p in range(n_kv):
-        proj_send[p] = proj[p * seqs : (p + 1) * seqs, :].astype(BF16)
+
+    def scatter(result, outgoing, incoming, sem):
+        for p in range(n_kv):
+            outgoing[p] = result[p * seqs : (p + 1) * seqs, :].astype(BF16)
+        exchange("kv", kv_me, n_kv, lambda p: outgoing.at[p], incoming, sem)
+        incoming[kv_me] = outgoing[kv_me]
+
+    project(early, 0, "wq", wq)
+    project(early, kw, "wk", wk)
     pl.semaphore_wait(barrier, n_kv + n_tp - 2)
-    pending += exchange("kv", kv_me, n_kv, lambda p: proj_send.at[p], proj_recv, send_a, recv_a)
-    proj_recv[kv_me] = proj_send[kv_me]
+    scatter(early, early_send, early_recv, 0)
+    project(proj, 0, "wv", wv)
+    project(proj, vw, "wg", wg)
+    scatter(proj, proj_send, proj_recv, 1)
 
     dw[rank:, :] = jnp.zeros((dw.shape[0] - rank, dw.shape[1]), BF16)
-    ready("decay")
-    ready("key")
+    ready(*("lengths", "decay", "key"))
     positions = lax.broadcasted_iota(jnp.int32, (span, heads_here, key_dim), 0)
     for b in range(seqs):
         live = positions < lengths_s[b]
@@ -255,17 +268,19 @@
         keyed[b] = jnp.where(live, key[b].astype(F32) * jnp.exp(later), 0.0)
     ready(*("dw", "db", "head_gain", "state", "value"))
 
-    await_arrivals(kv_me, n_kv, proj_recv, recv_a)
-    total = proj_recv[0].astype(F32)
-    for p in range(1, n_kv):
-        total = total + proj_recv[p].astype(F32)
+    def gathered(incoming):
+        total = incoming[0].astype(F32)
+        for p in range(1, n_kv):
+            total = total + incoming[p].astype(F32)
+        return total
+
+    await_arrivals(n_kv, early_recv, 0)
+    total = gathered(early_recv)
     misc = total[:, base_misc:]
     squares = misc[:, rank : rank + 1] + misc[:, rank + 1 : rank + 2]
     inv_rms = lax.rsqrt(squares / width + EPS)
     queries = (total[:, :kw] * inv_rms * key_dim ** (-0.5)).astype(BF16).astype(F32)
     new_keys = (total[:, kw : 2 * kw] * inv_rms).astype(BF16).astype(F32)
-    new_values = (total[:, 2 * kw : 2 * kw + vw] * inv_rms).astype(BF16).astype(F32)
-    out_gate = (total[:, 2 * kw + vw : base_misc] * inv_rms).astype(BF16).astype(F32)
     code = (misc * inv_rms).astype(BF16)
     pre_gate = dot(code, dw[...]) + db[...]
     new_decay = (jnp.minimum(pre_gate, 0.0) - jnp.log1p(jnp.exp(-jnp.abs(pre_gate)))) / GATE_TEMP
@@ -273,12 +288,9 @@
     for b in range(seqs):
         for h in range(heads_here):
             k_cols = slice(h * key_dim, (h + 1) * key_dim)
-            v_cols = slice(h * value_dim, (h + 1) * value_dim)
             decayed3[b, h : h + 1, :] = decayed[b : b + 1, k_cols]
             keys3[b, h : h + 1, :] = new_keys[b : b + 1, k_cols]
-            values3[b, h : h + 1, :] = new_values[b : b + 1, v_cols]
     nk_ref[...] = keys3[...].astype(BF16)
-    nv_ref[...] = values3[...].astype(BF16)
     for b in range(seqs):
         d = decayed3[b]
         scores = jnp.sum(keyed[b] * d[None], axis=-1, keepdims=True)
@@ -292,6 +304,10 @@
         for h in range(heads_here):
             carried = jnp.sum(into_state[:, h : h + 1] * state[b, h], axis=0, keepdims=True)
             mixed[b : b + 1, h * value_dim : (h + 1) * value_dim] = carried + within[h : h + 1]
+    await_arrivals(n_kv, proj_recv, 1)
+    total = gathered(proj_recv)
+    new_values = (total[:, :vw] * inv_rms).astype(BF16).astype(F32)
+    out_gate = (total[:, vw:] * inv_rms).astype(BF16).astype(F32)
     for h in range(heads_here):
         k_cols = slice(h * key_dim, (h + 1) * key_dim)
         v_cols = slice(h * value_dim, (h + 1) * value_dim)
@@ -301,21 +317,22 @@
         g = out_gate[:, v_cols]
         mixed[:, v_cols] = full * norm * head_gain[...] * (g / (1.0 + jnp.exp(-g)))
     heads_all[kv_me] = mixed[...].astype(BF16)
-    pending += exchange(
-        "kv", kv_me, n_kv, lambda p: heads_all.at[kv_me], heads_all, send_b, recv_b
-    )
+    exchange("kv", kv_me, n_kv, lambda p: heads_all.at[kv_me], heads_all, 2)
+    for b in range(seqs):
+        for h in range(heads_here):
+            v_cols = slice(h * value_dim, (h + 1) * value_dim)
+            values3[b, h : h + 1, :] = new_values[b : b + 1, v_cols]
+    nv_ref[...] = values3[...].astype(BF16)
 
     ready("wo")
     ready("mlp_gain")
-    await_arrivals(kv_me, n_kv, heads_all, recv_b)
+    await_arrivals(n_kv, heads_all, 2)
     for p in range(n_kv):
         heads[p * seqs : (p + 1) * seqs, :] = heads_all[p].astype(F32)
     attended[tp_me] = dot(heads[...].astype(BF16), wo[...]).astype(BF16)
-    pending += exchange(
-        "tp", tp_me, n_tp, lambda p: attended.at[tp_me], attended, send_c, recv_c
-    )
+    exchange("tp", tp_me, n_tp, lambda p: attended.at[tp_me], attended, 3)
     ready("gate")
-    await_arrivals(tp_me, n_tp, attended, recv_c)
+    await_arrivals(n_tp, attended, 3)
     summed = attended[0].astype(F32)
     for p in range(1, n_tp):
         summed = summed + attended[p].astype(F32)
@@ -340,40 +357,36 @@
             mlp_acc[:, size + 1 : size + 2] = low
         for p in range(n_kv):
             sends[part][p] = mlp_acc[p * seqs : (p + 1) * seqs, :].astype(BF16)
-        pending += exchange(
+        exchange(
             "kv",
             kv_me,
             n_kv,
             lambda p, part=part: sends[part].at[p],
             recvs[part],
-            send_d.at[part],
-            recv_d.at[part],
+            SHARED_SEMS + part,
         )
         recvs[part][kv_me] = sends[part][kv_me]
     for part, (first, size, span_cols) in enumerate(pieces):
-        await_arrivals(kv_me, n_kv, recvs[part], recv_d.at[part])
-        total = recvs[part][0].astype(F32)
-        for p in range(1, n_kv):
-            total = total + recvs[part][p].astype(F32)
+        await_arrivals(n_kv, recvs[part], SHARED_SEMS + part)
+        total = gathered(recvs[part])
         if part == 0:
             squares = total[:, size : size + 1] + total[:, size + 1 : size + 2]
             inv_mid = lax.rsqrt(squares / width + EPS)
         g = total[:, :span_cols] * inv_mid
         mine = g / (1.0 + jnp.exp(-g)) * (total[:, span_cols:] * inv_mid)
         hiddens_all[part][kv_me] = mine.astype(BF16)
-        pending += exchange(
+        exchange(
             "kv",
             kv_me,
             n_kv,
             lambda p, part=part: hiddens_all[part].at[kv_me],
             hiddens_all[part],
-            send_e.at[part],
-            recv_e.at[part],
+            SHARED_SEMS + PARTS + part,
         )
     ready("down")
     acc = jnp.zeros((rows, feats), F32)
     for part, (first, size, span_cols) in enumerate(pieces):
-        await_arrivals(kv_me, n_kv, hiddens_all[part], recv_e.at[part])
+        await_arrivals(n_kv, hiddens_all[part], SHARED_SEMS + PARTS + part)
         hidden = hiddens[part]
         for p in range(n_kv):
             hidden[p * seqs : (p + 1) * seqs, :] = hiddens_all[part][p].astype(F32)
@@ -384,14 +397,14 @@
             whole = hidden[...].astype(BF16)
         acc = acc + dot(whole, down[first : first + span_cols, :])
     lifted[tp_me] = acc.astype(BF16)
-    pending += exchange("tp", tp_me, n_tp, lambda p: lifted.at[tp_me], lifted, send_f, recv_f)
-    await_arrivals(tp_me, n_tp, lifted, recv_f)
+    exchange("tp", tp_me, n_tp, lambda p: lifted.at[tp_me], lifted, 4)
+    await_arrivals(n_tp, lifted, 4)
     summed = lifted[0].astype(F32)
     for p in range(1, n_tp):
         summed = summed + lifted[p].astype(F32)
     out_ref[...] = (mid_f + summed).astype(BF16)
-    for copy in pending:
-        copy.wait_send()
+    for ref, sem in pending:
+        drain(ref, send_sem.at[sem])
 
 
 def on_device(n_kv, n_tp, *args):
@@ -447,18 +460,22 @@
     units = gate.shape[1]
     rank = wc.shape[1]
     widths = [piece[2] for piece in pieces_of(units)]
-    cols = 2 * kw + 2 * vw + LANES
+    first_cols = 2 * kw + LANES
+    cols = 2 * vw
     vmem = pltpu.VMEM
 
     def copied(a):
         if a is lengths:
-            return None
+            return pltpu.SMEM(a.shape, a.dtype)
         if a is dw:
             return vmem((LANES, a.shape[1]), a.dtype)
         return vmem(a.shape, a.dtype)
 
-    scratch = [c for c in map(copied, operands) if c is not None]
+    scratch = [copied(a) for a in operands]
     scratch += [
+        vmem((rows, first_cols), F32),
+        vmem((n_kv, seqs, first_cols), BF16),
+        vmem((n_kv, seqs, first_cols), BF16),
         vmem((rows, cols), F32),
         vmem((n_kv, seqs, cols), BF16),
         vmem((n_kv, seqs, cols), BF16),
@@ -479,15 +496,9 @@
         vmem((n_tp, rows, feats), BF16),
     ]
     dma = pltpu.SemaphoreType.DMA
-    scratch += [dma((19,))]
-    scratch += [dma((n_kv,))] * 4
-    scratch += [dma((n_tp,))] * 2
-    scratch += [dma((PARTS, n_kv))] * 4
-    scratch += [dma((n_tp,))] * 2
-    hbm_spec = pl.BlockSpec(memory_space=pltpu.HBM)
-    in_specs = [
-        pl.BlockSpec(memory_space=pltpu.SMEM) if a is lengths else hbm_spec for a in operands
-    ]
+    scratch += [dma((len(operands),))]
+    scratch += [dma((SHARED_SEMS + 2 * PARTS,))] * 2
+    in_specs = [pl.BlockSpec(memory_space=pltpu.HBM)] * len(operands)
     shapes = ((rows, feats), (seqs, heads_here, key_dim), (seqs, heads_here, value_dim))
     results = pl.pallas_call(
         functools.partial(layer_kernel, n_kv, n_tp, feats * n_kv),
@@ -500,12 +511,11 @@
         ),
         name="layer",
     )(*operands)
-    local = (pl.BlockSpec(memory_space=pl.ANY),) * 3
     return pl.pallas_call(
         copy_out,
         out_shape=tuple(jax.ShapeDtypeStruct(shape, BF16) for shape in shapes),
-        in_specs=local,
-        out_specs=local,
+        in_specs=(pl.BlockSpec(memory_space=pltpu.VMEM),) * 3,
+        out_specs=(pl.BlockSpec(memory_space=pl.ANY),) * 3,
         scratch_shapes=[dma((3,))],
         name="results",
     )(*results)

time: 45.3 us -> 42.5 us (0.938)
  Pallas kernels: 42.7 us -> 39.9 us
    pallas_call x1, Pallas kernels: 40.4 us -> 38.5 us  [on_device(): pl.pallas_call(functools.partial(layer_kernel, n_kv, n_tp, feats * n_kv),...]
    pallas_call x1, Pallas kernels: 2.3 us -> 1.41 us  [on_device(): pl.pallas_call(copy_out, out_shape=tuple((jax.ShapeDtypeStruct(shape, BF1...]
where the time goes in v1:
time: 42.5 us; the launch traced here: 42.3 us
  Pallas kernels  39.9 us (94%)
  local copies, waits for them, and re-layouts  1.78 us (4%)
  between operations  0.66 us (2%)
    pallas_call x1, Pallas kernels, on_device(): pl.pallas_call(functools.partial(layer_kernel, n_kv, n_tp, feats * n_kv),...  38.5 us
    unnamed x6, local copies, waits for them, and re-layouts  1.78 us
    pallas_call x1, Pallas kernels, on_device(): pl.pallas_call(copy_out, out_shape=tuple((jax.ShapeDtypeStruct(shape, BF1...  1.41 us

profile of v1, /device:TPU:0, one launch (start us, length us, event | category | flops | bytes accessed | tf_op | source)
XLA Modules:
  0.0 42.3 jit_solution(16608137436201985844)
XLA Ops:
  0.6 38.5 %layer.1 = (bf16[32,512]{1,0:T(8,128)(2,1)S(1)}, bf16[4,2,128]{2,1,0:T(2,128)(2,1)S(1)}, bf16[4,2,256]{2,1,0:T(2,128)(2,1)S(1)}) custom-call(bf16[32,512]{1,0:T(8,128)(2,1)} %tokens_h.1, f32[1,512]{1,0:T(1,128)} %bitcast.10, bf16[512,256]{1,0:T(8,128)(2,1)} %wq_h.1, bf16[512,256]{1,0:T(8,128)(2,1)} %wk_h.1, bf16[512,512]{1,0:T(8,128)(2,1)} %wv_h.1, ...), custom_call_target="tpu_custom_call" | custom-call | tf_op jit(solution)/shard_map/layer/pallas_call | solution.py:503
  39.1 0.0 copy-start
  39.2 0.6 %copy-done = bf16[32,512]{1,0:T(8,128)(2,1)} copy-done((bf16[32,512]{1,0:T(8,128)(2,1)}, bf16[32,512]{1,0:T(8,128)(2,1)S(1)}, u32[]{:S(2)}) %copy-start) | copy-done | bytes 32792
  39.7 0.0 copy-start.2
  39.7 0.6 %copy-done.2 = bf16[4,2,128]{2,1,0:T(2,128)(2,1)} copy-done((bf16[4,2,128]{2,1,0:T(2,128)(2,1)}, bf16[4,2,128]{2,1,0:T(2,128)(2,1)S(1)}, u32[]{:S(2)}) %copy-start.2) | copy-done | bytes 2072
  40.3 0.0 copy-start.1
  40.3 0.6 %copy-done.1 = bf16[4,2,256]{2,1,0:T(2,128)(2,1)} copy-done((bf16[4,2,256]{2,1,0:T(2,128)(2,1)}, bf16[4,2,256]{2,1,0:T(2,128)(2,1)S(1)}, u32[]{:S(2)}) %copy-start.1) | copy-done | bytes 4120
  40.9 1.4 %results.1 = (bf16[32,512]{1,0:T(8,128)(2,1)}, bf16[4,2,128]{2,1,0:T(2,128)(2,1)}, bf16[4,2,256]{2,1,0:T(2,128)(2,1)}) custom-call(bf16[32,512]{1,0:T(8,128)(2,1)} %copy-done, bf16[4,2,128]{2,1,0:T(2,128)(2,1)} %copy-done.2, bf16[4,2,256]{2,1,0:T(2,128)(2,1)} %copy-done.1), custom_call_target="tpu_custom_call" | custom-call | tf_op jit(solution)/shard_map/results/pallas_call | solution.py:514
Async XLA Ops:
  39.1 0.6 %copy-start = (bf16[32,512]{1,0:T(8,128)(2,1)}, bf16[32,512]{1,0:T(8,128)(2,1)S(1)}, u32[]{:S(2)}) copy-start(bf16[32,512]{1,0:T(8,128)(2,1)S(1)} %get-tuple-element.6.refs_0_) | copy-start | bytes 98308
  39.7 0.6 %copy-start.2 = (bf16[4,2,128]{2,1,0:T(2,128)(2,1)}, bf16[4,2,128]{2,1,0:T(2,128)(2,1)S(1)}, u32[]{:S(2)}) copy-start(bf16[4,2,128]{2,1,0:T(2,128)(2,1)S(1)} %get-tuple-element.7.refs_1_) | copy-start | bytes 6148
  40.3 0.6 %copy-start.1 = (bf16[4,2,256]{2,1,0:T(2,128)(2,1)}, bf16[4,2,256]{2,1,0:T(2,128)(2,1)S(1)}, u32[]{:S(2)}) copy-start(bf16[4,2,256]{2,1,0:T(2,128)(2,1)S(1)} %get-tuple-element.8.refs_2_) | copy-start | bytes 12292

commit v2 on v1

--- a/solution.py
+++ b/solution.py
@@ -10,9 +10,12 @@
 EPS = 1e-06
 GATE_TEMP = 16.0
 FIRST_LOADS = 7
-PARTS = 4
-SHARED_SEMS = 5
+SHARES = (4, 6, 7, 5)
+PARTS = len(SHARES)
 LANES = 128
+SWAPPED_LOADS = ("decay", "key", "dw", "db", "state", "value")
+SEM_EARLY, SEM_PROJ, SEM_HEADS, SEM_ATTEND, SEM_LIFT, SEM_KEYS, SEM_VALUES = range(7)
+SHARED_SEMS = 7
 F32 = jnp.float32
 BF16 = jnp.bfloat16
 
@@ -35,10 +38,16 @@
 
 
 def pieces_of(units):
-    each = units // PARTS // LANES * LANES
-    head = units - (PARTS - 1) * each
+    blocks = units // LANES
+    counts = [share * blocks // sum(SHARES) for share in SHARES]
+    counts[0] = blocks - sum(counts[1:])
+    head = units - LANES * sum(counts[1:])
     room = (head + 2 + LANES - 1) // LANES * LANES
-    return [(0, head, room)] + [(head + k * each, each, each) for k in range(PARTS - 1)]
+    pieces, first = [(0, head, room)], head
+    for count in counts[1:]:
+        pieces.append((first, count * LANES, count * LANES))
+        first += count * LANES
+    return pieces
 
 
 def peer_of(me, step, count):
@@ -54,6 +63,11 @@
 
 def drain(ref, sem):
     pltpu.make_async_copy(ref, ref, sem).wait()
+
+
+def stacked(array, parts):
+    width = array.shape[1] // parts
+    return jnp.concatenate([array[:, k * width : (k + 1) * width] for k in range(parts)], axis=0)
 
 
 def copy_out(*refs):
@@ -122,11 +136,15 @@
     proj_send,
     proj_recv,
     keyed,
+    keyed_rows,
+    value_rows,
+    state_rows,
     total_exp,
-    decayed3,
-    keys3,
-    values3,
-    mixed,
+    keys_send,
+    keys_recv,
+    values_send,
+    values_recv,
+    heads_send,
     heads,
     heads_all,
     attended,
@@ -134,6 +152,7 @@
     sends,
     recvs,
     hiddens,
+    hidden_sends,
     hiddens_all,
     lifted,
     load_sem,
@@ -142,6 +161,7 @@
 ):
     kv_me = lax.axis_index("kv")
     tp_me = lax.axis_index("tp")
+    tp_mate = tp_me + 1 - 2 * lax.rem(tp_me, 2)
     rows, feats = tokens.shape
     seqs, span, heads_here, key_dim = key.shape
     value_dim = value.shape[3]
@@ -164,57 +184,75 @@
         ("key", key_h, key),
         ("dw", dw_h, dw.at[pl.ds(0, rank)]),
         ("db", db_h, db),
-        ("head_gain", head_gain_h, head_gain),
         ("state", state_h, state),
         ("value", value_h, value),
+        ("head_gain", head_gain_h, head_gain),
         ("wo", wo_h, wo),
         ("mlp_gain", mlp_gain_h, mlp_gain),
         ("gate", gate_h, gate),
         ("up", up_h, up),
         ("down", down_h, down),
     ]
+    given = []
     for place, (name, source, target) in enumerate(pairs):
-        loads[name] = pltpu.make_async_copy(source, target, load_sem.at[place])
+        if name in SWAPPED_LOADS:
+            loads[name] = pltpu.make_async_remote_copy(
+                src_ref=source,
+                dst_ref=target,
+                send_sem=load_sem.at[len(pairs) + len(given)],
+                recv_sem=load_sem.at[place],
+                device_id={"tp": tp_mate},
+                device_id_type=pl.DeviceIdType.MESH,
+            )
+            given.append(loads[name])
+        else:
+            loads[name] = pltpu.make_async_copy(source, target, load_sem.at[place])
         if place < FIRST_LOADS:
             loads[name].start()
 
     def ready(*names):
         for name in names:
-            loads.pop(name).wait()
+            load = loads.pop(name)
+            if name in SWAPPED_LOADS:
+                load.wait_recv()
+            else:
+                load.wait()
 
     barrier = pltpu.get_barrier_semaphore()
-    for off in range(1, n_kv):
+    others = [{"kv": peer_of(kv_me, k, n_kv), "tp": tp_mate} for k in range(n_kv)]
+    others += [{"tp": lax.rem(tp_mate + 2 * k, n_tp)} for k in range(1, n_tp // 2)]
+    others += [{"tp": lax.rem(tp_me + 2 * k, n_tp)} for k in range(1, n_tp // 2)]
+    for other in others:
         pl.semaphore_signal(
-            barrier,
-            inc=1,
-            device_id={"kv": lax.rem(kv_me + off, n_kv)},
+            barrier, inc=1, device_id=other, device_id_type=pl.DeviceIdType.MESH
+        )
+
+    pending = []
+
+    def send(source, target, sem, device):
+        pltpu.make_async_remote_copy(
+            src_ref=source,
+            dst_ref=target,
+            send_sem=send_sem.at[sem],
+            recv_sem=recv_sem.at[sem],
+            device_id=device,
             device_id_type=pl.DeviceIdType.MESH,
-        )
-    for off in range(1, n_tp):
-        pl.semaphore_signal(
-            barrier,
-            inc=1,
-            device_id={"tp": lax.rem(tp_me + off, n_tp)},
-            device_id_type=pl.DeviceIdType.MESH,
-        )
-
-    pending = []
-
-    def exchange(axis, me, count, source, target, sem):
-        for step in range(count - 1, 0, -1):
-            p = peer_of(me, step, count)
-            pltpu.make_async_remote_copy(
-                src_ref=source(p),
-                dst_ref=target.at[me],
-                send_sem=send_sem.at[sem],
-                recv_sem=recv_sem.at[sem],
-                device_id={axis: p},
-                device_id_type=pl.DeviceIdType.MESH,
-            ).start()
-        pending.append((target.at[pl.ds(0, count - 1)], sem))
-
-    def await_arrivals(count, target, sem):
-        drain(target.at[pl.ds(0, count - 1)], recv_sem.at[sem])
+        ).start()
+
+    def to_kv(source, target, sem):
+        for step in range(n_kv - 1, -1, -1):
+            p = peer_of(kv_me, step, n_kv)
+            send(source(p), target.at[kv_me], sem, {"kv": p, "tp": tp_mate})
+        pending.append((target, sem))
+
+    def to_tp(target, sem):
+        for step in range(n_tp - 1, 0, -1):
+            p = peer_of(tp_me, step, n_tp)
+            send(target.at[tp_me], target.at[tp_me], sem, {"tp": p})
+        pending.append((target.at[pl.ds(0, n_tp - 1)], sem))
+
+    def await_tp(target, sem):
+        drain(target.at[pl.ds(0, n_tp - 1)], recv_sem.at[sem])
 
     base_misc = 2 * kw
     ready(*("tokens", "attn_gain", "wc"))
@@ -228,9 +266,6 @@
 
     def project(result, base, name, weight):
         ready(name)
-        if name == "wg":
-            for late in list(loads.values()):
-                late.start()
         for start, size in tiles_of(weight.shape[1], 256):
             result[:, base + start : base + start + size] = dot(
                 scaled, weight[:, start : start + size]
@@ -239,16 +274,21 @@
     def scatter(result, outgoing, incoming, sem):
         for p in range(n_kv):
             outgoing[p] = result[p * seqs : (p + 1) * seqs, :].astype(BF16)
-        exchange("kv", kv_me, n_kv, lambda p: outgoing.at[p], incoming, sem)
-        incoming[kv_me] = outgoing[kv_me]
+        to_kv(lambda p: outgoing.at[p], incoming, sem)
 
     project(early, 0, "wq", wq)
     project(early, kw, "wk", wk)
-    pl.semaphore_wait(barrier, n_kv + n_tp - 2)
-    scatter(early, early_send, early_recv, 0)
+    pl.semaphore_wait(barrier, len(others))
+    scatter(early, early_send, early_recv, SEM_EARLY)
+    loads["lengths"].start()
+    for load in given:
+        load.start()
     project(proj, 0, "wv", wv)
     project(proj, vw, "wg", wg)
-    scatter(proj, proj_send, proj_recv, 1)
+    scatter(proj, proj_send, proj_recv, SEM_PROJ)
+    for name, load in loads.items():
+        if name not in SWAPPED_LOADS and name != "lengths":
+            load.start()
 
     dw[rank:, :] = jnp.zeros((dw.shape[0] - rank, dw.shape[1]), BF16)
     ready(*("lengths", "decay", "key"))
@@ -263,10 +303,21 @@
                 [suffix[step:], jnp.zeros((step, heads_here, key_dim), F32)], axis=0
             )
             step *= 2
-        total_exp[b] = jnp.exp(suffix[0])
+        for h in range(heads_here):
+            total_exp[h * seqs + b : h * seqs + b + 1, :] = jnp.exp(suffix[0, h : h + 1])
         later = jnp.concatenate([suffix[1:], jnp.zeros((1, heads_here, key_dim), F32)], axis=0)
         keyed[b] = jnp.where(live, key[b].astype(F32) * jnp.exp(later), 0.0)
+    for b in range(seqs):
+        for h in range(heads_here):
+            r = h * seqs + b
+            keyed_rows[r * span : (r + 1) * span, :] = keyed[b, :, h, :].astype(BF16)
     ready(*("dw", "db", "head_gain", "state", "value"))
+    for b in range(seqs):
+        block = value[b].astype(F32)
+        for h in range(heads_here):
+            r = h * seqs + b
+            value_rows[r * span : (r + 1) * span, :] = block[:, h, :].astype(BF16)
+            state_rows[r * key_dim : (r + 1) * key_dim, :] = state[b, h].astype(BF16)
 
     def gathered(incoming):
         total = incoming[0].astype(F32)
@@ -274,72 +325,78 @@
             total = total + incoming[p].astype(F32)
         return total
 
-    await_arrivals(n_kv, early_recv, 0)
+    drain(early_recv, recv_sem.at[SEM_EARLY])
     total = gathered(early_recv)
     misc = total[:, base_misc:]
     squares = misc[:, rank : rank + 1] + misc[:, rank + 1 : rank + 2]
     inv_rms = lax.rsqrt(squares / width + EPS)
     queries = (total[:, :kw] * inv_rms * key_dim ** (-0.5)).astype(BF16).astype(F32)
-    new_keys = (total[:, kw : 2 * kw] * inv_rms).astype(BF16).astype(F32)
+    new_keys = (total[:, kw : 2 * kw] * inv_rms).astype(BF16)
+    keys_send[...] = new_keys
+    send(keys_send, keys_recv, SEM_KEYS, {"tp": tp_mate})
+    pending.append((keys_send, SEM_KEYS))
     code = (misc * inv_rms).astype(BF16)
     pre_gate = dot(code, dw[...]) + db[...]
     new_decay = (jnp.minimum(pre_gate, 0.0) - jnp.log1p(jnp.exp(-jnp.abs(pre_gate)))) / GATE_TEMP
-    decayed = queries * jnp.exp(new_decay)
-    for b in range(seqs):
-        for h in range(heads_here):
-            k_cols = slice(h * key_dim, (h + 1) * key_dim)
-            decayed3[b, h : h + 1, :] = decayed[b : b + 1, k_cols]
-            keys3[b, h : h + 1, :] = new_keys[b : b + 1, k_cols]
-    nk_ref[...] = keys3[...].astype(BF16)
-    for b in range(seqs):
-        d = decayed3[b]
-        scores = jnp.sum(keyed[b] * d[None], axis=-1, keepdims=True)
-        scores = scores.astype(BF16).astype(F32)
-        within = jnp.sum(scores * value[b].astype(F32), axis=0)
-        into_state = jnp.transpose(
-            jnp.concatenate(
-                [d * total_exp[b], jnp.zeros((8 - heads_here, key_dim), F32)], axis=0
-            )
-        )
-        for h in range(heads_here):
-            carried = jnp.sum(into_state[:, h : h + 1] * state[b, h], axis=0, keepdims=True)
-            mixed[b : b + 1, h * value_dim : (h + 1) * value_dim] = carried + within[h : h + 1]
-    await_arrivals(n_kv, proj_recv, 1)
+    pairs_here = heads_here * seqs
+    decayed = stacked(queries * jnp.exp(new_decay), heads_here)
+    own = jnp.sum(
+        stacked(queries, heads_here) * stacked(new_keys.astype(F32), heads_here),
+        axis=-1,
+        keepdims=True,
+    )
+
+    def own_block(wide):
+        each = wide.shape[1] // pairs_here
+        pair = lax.broadcasted_iota(jnp.int32, wide.shape, 0)
+        place = lax.broadcasted_iota(jnp.int32, wide.shape, 1)
+        mine = (place >= pair * each) & (place < (pair + 1) * each)
+        return jnp.where(mine, wide, 0.0).astype(BF16)
+
+    into_state = decayed * total_exp[...]
+    carried = dot(own_block(jnp.concatenate([into_state] * pairs_here, axis=1)), state_rows[...])
+    scores = own_block(dot_t(decayed.astype(BF16), keyed_rows[...]))
+    full = carried + dot(scores, value_rows[...])
+    drain(proj_recv, recv_sem.at[SEM_PROJ])
     total = gathered(proj_recv)
-    new_values = (total[:, :vw] * inv_rms).astype(BF16).astype(F32)
+    new_values = (total[:, :vw] * inv_rms).astype(BF16)
     out_gate = (total[:, vw:] * inv_rms).astype(BF16).astype(F32)
+    full = full + own * stacked(new_values.astype(F32), heads_here)
+    norm = lax.rsqrt(jnp.mean(full * full, axis=-1, keepdims=True) + EPS)
+    g = stacked(out_gate, heads_here)
+    mixed = full * norm * head_gain[...] * (g / (1.0 + jnp.exp(-g)))
     for h in range(heads_here):
-        k_cols = slice(h * key_dim, (h + 1) * key_dim)
-        v_cols = slice(h * value_dim, (h + 1) * value_dim)
-        own = jnp.sum(queries[:, k_cols] * new_keys[:, k_cols], axis=-1, keepdims=True)
-        full = mixed[:, v_cols] + own * new_values[:, v_cols]
-        norm = lax.rsqrt(jnp.mean(full * full, axis=-1, keepdims=True) + EPS)
-        g = out_gate[:, v_cols]
-        mixed[:, v_cols] = full * norm * head_gain[...] * (g / (1.0 + jnp.exp(-g)))
-    heads_all[kv_me] = mixed[...].astype(BF16)
-    exchange("kv", kv_me, n_kv, lambda p: heads_all.at[kv_me], heads_all, 2)
-    for b in range(seqs):
-        for h in range(heads_here):
-            v_cols = slice(h * value_dim, (h + 1) * value_dim)
-            values3[b, h : h + 1, :] = new_values[b : b + 1, v_cols]
-    nv_ref[...] = values3[...].astype(BF16)
-
+        heads_send[:, h * value_dim : (h + 1) * value_dim] = mixed[
+            h * seqs : (h + 1) * seqs
+        ].astype(BF16)
+    to_kv(lambda p: heads_send, heads_all, SEM_HEADS)
+    values_send[...] = new_values
+    send(values_send, values_recv, SEM_VALUES, {"tp": tp_mate})
+    pending.append((values_send, SEM_VALUES))
     ready("wo")
     ready("mlp_gain")
-    await_arrivals(n_kv, heads_all, 2)
+    drain(heads_all, recv_sem.at[SEM_HEADS])
     for p in range(n_kv):
         heads[p * seqs : (p + 1) * seqs, :] = heads_all[p].astype(F32)
     attended[tp_me] = dot(heads[...].astype(BF16), wo[...]).astype(BF16)
-    exchange("tp", tp_me, n_tp, lambda p: attended.at[tp_me], attended, 3)
+    to_tp(attended, SEM_ATTEND)
+    drain(keys_recv, recv_sem.at[SEM_KEYS])
+    drain(values_recv, recv_sem.at[SEM_VALUES])
+    for h in range(heads_here):
+        keys = keys_recv[:, h * key_dim : (h + 1) * key_dim].astype(F32)
+        values = values_recv[:, h * value_dim : (h + 1) * value_dim].astype(F32)
+        for b in range(seqs):
+            nk_ref[b, h : h + 1, :] = keys[b : b + 1].astype(BF16)
+            nv_ref[b, h : h + 1, :] = values[b : b + 1].astype(BF16)
     ready("gate")
-    await_arrivals(n_tp, attended, 3)
+    ready("up")
+    await_tp(attended, SEM_ATTEND)
     summed = attended[0].astype(F32)
     for p in range(1, n_tp):
         summed = summed + attended[p].astype(F32)
     mid_f = (token_f + summed).astype(BF16).astype(F32)
     scaled_mid = (mid_f * mlp_gain[...]).astype(BF16)
 
-    ready("up")
     for part, (first, size, span_cols) in enumerate(pieces):
         mlp_acc = accs[part]
         for base, weight in ((0, gate), (span_cols, up)):
@@ -355,38 +412,23 @@
             high, low = split_sum(jnp.sum(mid_f * mid_f, axis=1, keepdims=True))
             mlp_acc[:, size : size + 1] = high
             mlp_acc[:, size + 1 : size + 2] = low
-        for p in range(n_kv):
-            sends[part][p] = mlp_acc[p * seqs : (p + 1) * seqs, :].astype(BF16)
-        exchange(
-            "kv",
-            kv_me,
-            n_kv,
-            lambda p, part=part: sends[part].at[p],
-            recvs[part],
-            SHARED_SEMS + part,
-        )
-        recvs[part][kv_me] = sends[part][kv_me]
+        scatter(mlp_acc, sends[part], recvs[part], SHARED_SEMS + part)
     for part, (first, size, span_cols) in enumerate(pieces):
-        await_arrivals(n_kv, recvs[part], SHARED_SEMS + part)
+        drain(recvs[part], recv_sem.at[SHARED_SEMS + part])
         total = gathered(recvs[part])
         if part == 0:
             squares = total[:, size : size + 1] + total[:, size + 1 : size + 2]
             inv_mid = lax.rsqrt(squares / width + EPS)
         g = total[:, :span_cols] * inv_mid
         mine = g / (1.0 + jnp.exp(-g)) * (total[:, span_cols:] * inv_mid)
-        hiddens_all[part][kv_me] = mine.astype(BF16)
-        exchange(
-            "kv",
-            kv_me,
-            n_kv,
-            lambda p, part=part: hiddens_all[part].at[kv_me],
-            hiddens_all[part],
-            SHARED_SEMS + PARTS + part,
+        hidden_sends[part][...] = mine.astype(BF16)
+        to_kv(
+            lambda p, part=part: hidden_sends[part], hiddens_all[part], SHARED_SEMS + PARTS + part
         )
     ready("down")
     acc = jnp.zeros((rows, feats), F32)
     for part, (first, size, span_cols) in enumerate(pieces):
-        await_arrivals(n_kv, hiddens_all[part], SHARED_SEMS + PARTS + part)
+        drain(hiddens_all[part], recv_sem.at[SHARED_SEMS + PARTS + part])
         hidden = hiddens[part]
         for p in range(n_kv):
             hidden[p * seqs : (p + 1) * seqs, :] = hiddens_all[part][p].astype(F32)
@@ -397,12 +439,14 @@
             whole = hidden[...].astype(BF16)
         acc = acc + dot(whole, down[first : first + span_cols, :])
     lifted[tp_me] = acc.astype(BF16)
-    exchange("tp", tp_me, n_tp, lambda p: lifted.at[tp_me], lifted, 4)
-    await_arrivals(n_tp, lifted, 4)
+    to_tp(lifted, SEM_LIFT)
+    await_tp(lifted, SEM_LIFT)
     summed = lifted[0].astype(F32)
     for p in range(1, n_tp):
         summed = summed + lifted[p].astype(F32)
     out_ref[...] = (mid_f + summed).astype(BF16)
+    for load in given:
+        load.wait_send()
     for ref, sem in pending:
         drain(ref, send_sem.at[sem])
 
@@ -457,8 +501,8 @@
     seqs, span, heads_here, key_dim = key.shape
     value_dim = value.shape[3]
     kw, vw = heads_here * key_dim, heads_here * value_dim
+    pairs = heads_here * seqs
     units = gate.shape[1]
-    rank = wc.shape[1]
     widths = [piece[2] for piece in pieces_of(units)]
     first_cols = 2 * kw + LANES
     cols = 2 * vw
@@ -480,11 +524,15 @@
         vmem((n_kv, seqs, cols), BF16),
         vmem((n_kv, seqs, cols), BF16),
         vmem((seqs, span, heads_here, key_dim), F32),
-        vmem((seqs, heads_here, key_dim), F32),
-        vmem((seqs, heads_here, key_dim), F32),
-        vmem((seqs, heads_here, key_dim), F32),
-        vmem((seqs, heads_here, value_dim), F32),
-        vmem((seqs, vw), F32),
+        vmem((pairs * span, key_dim), BF16),
+        vmem((pairs * span, value_dim), BF16),
+        vmem((pairs * key_dim, value_dim), BF16),
+        vmem((pairs, key_dim), F32),
+        vmem((seqs, kw), BF16),
+        vmem((seqs, kw), BF16),
+        vmem((seqs, vw), BF16),
+        vmem((seqs, vw), BF16),
+        vmem((seqs, vw), BF16),
         vmem((rows, vw), F32),
         vmem((n_kv, seqs, vw), BF16),
         vmem((n_tp, rows, feats), BF16),
@@ -492,11 +540,12 @@
         [vmem((n_kv, seqs, 2 * w), BF16) for w in widths],
         [vmem((n_kv, seqs, 2 * w), BF16) for w in widths],
         [vmem((rows, w), F32) for w in widths],
+        [vmem((seqs, w), BF16) for w in widths],
         [vmem((n_kv, seqs, w), BF16) for w in widths],
         vmem((n_tp, rows, feats), BF16),
     ]
     dma = pltpu.SemaphoreType.DMA
-    scratch += [dma((len(operands),))]
+    scratch += [dma((len(operands) + len(SWAPPED_LOADS),))]
     scratch += [dma((SHARED_SEMS + 2 * PARTS,))] * 2
     in_specs = [pl.BlockSpec(memory_space=pltpu.HBM)] * len(operands)
     shapes = ((rows, feats), (seqs, heads_here, key_dim), (seqs, heads_here, value_dim))
@@ -518,7 +567,7 @@
         out_specs=(pl.BlockSpec(memory_space=pl.ANY),) * 3,
         scratch_shapes=[dma((3,))],
         name="results",
-    )(*results)
+    )(*(pltpu.with_memory_space_constraint(r, pltpu.VMEM) for r in results))
 
 
 def solution(mesh):

time: 42.5 us -> 38.3 us (0.901)
  Pallas kernels: 39.9 us -> 37.5 us
  local copies, waits for them, and re-layouts: 1.78 us -> 0 us
    unnamed x6 -> x0, local copies, waits for them, and re-layouts: 1.78 us -> none
    pallas_call x1, Pallas kernels: 38.5 us -> 36.8 us  [on_device(): pl.pallas_call(functools.partial(layer_kernel, n_kv, n_tp, feats * n_kv),...]
    pallas_call x1, Pallas kernels: 1.41 us -> 0.65 us  [on_device(): pl.pallas_call(copy_out, out_shape=tuple((jax.ShapeDtypeStruct(shape, BF1...]
where the time goes in v2:
time: 38.3 us; the launch traced here: 38.1 us
  Pallas kernels  37.5 us (98%)
  between operations  0.65 us (2%)
    pallas_call x1, Pallas kernels, on_device(): pl.pallas_call(functools.partial(layer_kernel, n_kv, n_tp, feats * n_kv),...  36.8 us

profile of v2, /device:TPU:0, one launch (start us, length us, event | category | flops | bytes accessed | tf_op | source)
XLA Modules:
  0.0 38.1 jit_solution(3335579271841713821)
XLA Ops:
  0.6 36.8 %layer.1 = (bf16[32,512]{1,0:T(8,128)(2,1)S(1)}, bf16[4,2,128]{2,1,0:T(2,128)(2,1)S(1)}, bf16[4,2,256]{2,1,0:T(2,128)(2,1)S(1)}) custom-call(bf16[32,512]{1,0:T(8,128)(2,1)} %tokens_h.1, f32[1,512]{1,0:T(1,128)} %bitcast.10, bf16[512,256]{1,0:T(8,128)(2,1)} %wq_h.1, bf16[512,256]{1,0:T(8,128)(2,1)} %wk_h.1, bf16[512,512]{1,0:T(8,128)(2,1)} %wv_h.1, ...), custom_call_target="tpu_custom_call" | custom-call | tf_op jit(solution)/shard_map/layer/pallas_call | solution.py:552
  37.5 0.6 %results.1 = (bf16[32,512]{1,0:T(8,128)(2,1)}, bf16[4,2,128]{2,1,0:T(2,128)(2,1)}, bf16[4,2,256]{2,1,0:T(2,128)(2,1)}) custom-call(bf16[32,512]{1,0:T(8,128)(2,1)S(1)} %get-tuple-element.6.refs_0_, bf16[4,2,128]{2,1,0:T(2,128)(2,1)S(1)} %get-tuple-element.7.refs_1_, bf16[4,2,256]{2,1,0:T(2,128)(2,1)S(1)} %get-tuple-element.8.refs_2_), custom_call_target="tpu_custom_call" | custom-call | tf_op jit(solution)/shard_map/results/pallas_call | solution.py:563

commit v3 on v2

--- a/solution.py
+++ b/solution.py
@@ -10,12 +10,16 @@
 EPS = 1e-06
 GATE_TEMP = 16.0
 FIRST_LOADS = 7
-SHARES = (4, 6, 7, 5)
+SHARES = (4, 6, 6, 6)
+COMPUTE = (0, 1, 2, 3)
+PAIRED = (1, 2)
+ORDER = (0, 3, 1, 2)
 PARTS = len(SHARES)
 LANES = 128
 SWAPPED_LOADS = ("decay", "key", "dw", "db", "state", "value")
-SEM_EARLY, SEM_PROJ, SEM_HEADS, SEM_ATTEND, SEM_LIFT, SEM_KEYS, SEM_VALUES = range(7)
-SHARED_SEMS = 7
+SEM_EARLY, SEM_PROJ, SEM_KEYS, SEM_VALUES = range(4)
+SEM_HEADS, SEM_ATTEND, SEM_LIFT, SEM_TAIL = 4, 6, 8, 10
+SHARED_SEMS = 11
 F32 = jnp.float32
 BF16 = jnp.bfloat16
 
@@ -51,14 +55,16 @@
 
 
 def peer_of(me, step, count):
-    if count & (count - 1):
-        return lax.rem(me + step, count)
     place, bit = 0, 1
     while bit < count:
         own = lax.rem(me // bit, 2)
         place = place + bit * (1 - own if step & bit else own)
         bit *= 2
     return place
+
+
+def slots_of(count):
+    return [3 * count // 4 if k in PAIRED else count for k in range(PARTS)]
 
 
 def drain(ref, sem):
@@ -86,6 +92,7 @@
     n_kv,
     n_tp,
     width,
+    heads_here,
     tokens_h,
     attn_gain_h,
     wq_h,
@@ -129,29 +136,28 @@
     gate,
     up,
     down,
+    scaled_mid,
     early,
     early_send,
     early_recv,
     proj,
     proj_send,
     proj_recv,
-    keyed,
     keyed_rows,
     value_rows,
-    state_rows,
     total_exp,
     keys_send,
     keys_recv,
     values_send,
     values_recv,
     heads_send,
-    heads,
     heads_all,
     attended,
     accs,
     sends,
     recvs,
-    hiddens,
+    mate_parts,
+    far_sends,
     hidden_sends,
     hiddens_all,
     lifted,
@@ -163,12 +169,18 @@
     tp_me = lax.axis_index("tp")
     tp_mate = tp_me + 1 - 2 * lax.rem(tp_me, 2)
     rows, feats = tokens.shape
-    seqs, span, heads_here, key_dim = key.shape
+    seqs, spread, key_dim = key.shape
     value_dim = value.shape[3]
     kw, vw = heads_here * key_dim, heads_here * value_dim
     rank = wc.shape[0]
     units = gate.shape[0]
     pieces = pieces_of(units)
+    side, half = lax.rem(kv_me, 2), n_kv // 4
+    local = lax.rem(kv_me // 2, half)
+    near = kv_me // 2 - local
+    far = half - near
+    bases, group = (near, far), rows // 2
+    slots = (local * 2 + side, 2 * half + local * 2 + side)
 
     loads = {}
     pairs = [
@@ -184,8 +196,8 @@
         ("key", key_h, key),
         ("dw", dw_h, dw.at[pl.ds(0, rank)]),
         ("db", db_h, db),
+        ("value", value_h, value),
         ("state", state_h, state),
-        ("value", value_h, value),
         ("head_gain", head_gain_h, head_gain),
         ("wo", wo_h, wo),
         ("mlp_gain", mlp_gain_h, mlp_gain),
@@ -222,6 +234,7 @@
     others = [{"kv": peer_of(kv_me, k, n_kv), "tp": tp_mate} for k in range(n_kv)]
     others += [{"tp": lax.rem(tp_mate + 2 * k, n_tp)} for k in range(1, n_tp // 2)]
     others += [{"tp": lax.rem(tp_me + 2 * k, n_tp)} for k in range(1, n_tp // 2)]
+    others.append({"kv": kv_me + 1 - 2 * side})
     for other in others:
         pl.semaphore_signal(
             barrier, inc=1, device_id=other, device_id_type=pl.DeviceIdType.MESH
@@ -239,11 +252,24 @@
             device_id_type=pl.DeviceIdType.MESH,
         ).start()
 
-    def to_kv(source, target, sem):
+    def to_kv(source, target, near_sem, far_sem):
         for step in range(n_kv - 1, -1, -1):
             p = peer_of(kv_me, step, n_kv)
-            send(source(p), target.at[kv_me], sem, {"kv": p, "tp": tp_mate})
-        pending.append((target, sem))
+            distant = step >= n_kv // 2
+            send(
+                source(p),
+                target.at[slots[distant]],
+                far_sem if distant else near_sem,
+                {"kv": p, "tp": tp_mate},
+            )
+        if near_sem == far_sem:
+            pending.append((target, near_sem))
+        else:
+            pending.append((target.at[pl.ds(0, 2 * half)], near_sem))
+            pending.append((target.at[pl.ds(0, 2 * half)], far_sem))
+
+    def await_kv(target, sem):
+        drain(target.at[pl.ds(0, 2 * half)], recv_sem.at[sem])
 
     def to_tp(target, sem):
         for step in range(n_tp - 1, 0, -1):
@@ -251,8 +277,16 @@
             send(target.at[tp_me], target.at[tp_me], sem, {"tp": p})
         pending.append((target.at[pl.ds(0, n_tp - 1)], sem))
 
-    def await_tp(target, sem):
+    def summed(target, sem):
         drain(target.at[pl.ds(0, n_tp - 1)], recv_sem.at[sem])
+        total = target[0].astype(F32)
+        for p in range(1, n_tp):
+            total = total + target[p].astype(F32)
+        return total
+
+    def rows_of(block):
+        start = bases[block] * 2 * seqs
+        return pl.ds(pl.multiple_of(start, group), group)
 
     base_misc = 2 * kw
     ready(*("tokens", "attn_gain", "wc"))
@@ -274,7 +308,7 @@
     def scatter(result, outgoing, incoming, sem):
         for p in range(n_kv):
             outgoing[p] = result[p * seqs : (p + 1) * seqs, :].astype(BF16)
-        to_kv(lambda p: outgoing.at[p], incoming, sem)
+        to_kv(lambda p: outgoing.at[p], incoming, sem, sem)
 
     project(early, 0, "wq", wq)
     project(early, kw, "wk", wk)
@@ -292,36 +326,48 @@
 
     dw[rank:, :] = jnp.zeros((dw.shape[0] - rank, dw.shape[1]), BF16)
     ready(*("lengths", "decay", "key"))
-    positions = lax.broadcasted_iota(jnp.int32, (span, heads_here, key_dim), 0)
+    positions = lax.broadcasted_iota(jnp.int32, (spread, key_dim), 0)
     for b in range(seqs):
-        live = positions < lengths_s[b]
+        live = positions < lengths_s[b] * heads_here
         kept = jnp.where(live, decay[b], 0.0)
         suffix = kept
-        step = 1
-        while step < span:
+        step = heads_here
+        while step < spread:
             suffix = suffix + jnp.concatenate(
-                [suffix[step:], jnp.zeros((step, heads_here, key_dim), F32)], axis=0
+                [suffix[step:], jnp.zeros((step, key_dim), F32)], axis=0
             )
             step *= 2
+        totals = jnp.exp(suffix[:heads_here])
         for h in range(heads_here):
-            total_exp[h * seqs + b : h * seqs + b + 1, :] = jnp.exp(suffix[0, h : h + 1])
-        later = jnp.concatenate([suffix[1:], jnp.zeros((1, heads_here, key_dim), F32)], axis=0)
-        keyed[b] = jnp.where(live, key[b].astype(F32) * jnp.exp(later), 0.0)
+            total_exp[h * seqs + b : h * seqs + b + 1, :] = totals[h : h + 1]
+        later = jnp.concatenate(
+            [suffix[heads_here:], jnp.zeros((heads_here, key_dim), F32)], axis=0
+        )
+        keyed_rows[b * spread : (b + 1) * spread, :] = jnp.where(
+            live, key[b].astype(F32) * jnp.exp(later), 0.0
+        ).astype(BF16)
+    ready(*("value", "dw", "db", "head_gain"))
     for b in range(seqs):
-        for h in range(heads_here):
-            r = h * seqs + b
-            keyed_rows[r * span : (r + 1) * span, :] = keyed[b, :, h, :].astype(BF16)
-    ready(*("dw", "db", "head_gain", "state", "value"))
-    for b in range(seqs):
-        block = value[b].astype(F32)
-        for h in range(heads_here):
-            r = h * seqs + b
-            value_rows[r * span : (r + 1) * span, :] = block[:, h, :].astype(BF16)
-            state_rows[r * key_dim : (r + 1) * key_dim, :] = state[b, h].astype(BF16)
+        value_rows[b * spread : (b + 1) * spread, :] = value[b].reshape(spread, value_dim)
+    pairs_here = heads_here * seqs
+    block_shape = (pairs_here, seqs * spread)
+    pair = lax.broadcasted_iota(jnp.int32, block_shape, 0)
+    place = lax.broadcasted_iota(jnp.int32, block_shape, 1)
+    begin = lax.rem(pair, seqs) * spread
+    score_mask = (
+        (place >= begin)
+        & (place < begin + spread)
+        & (lax.rem(place, heads_here) == pair // seqs)
+    )
+    wide_shape = (pairs_here, pairs_here * key_dim)
+    pair = lax.broadcasted_iota(jnp.int32, wide_shape, 0)
+    place = lax.broadcasted_iota(jnp.int32, wide_shape, 1)
+    begin = (lax.rem(pair, seqs) * heads_here + pair // seqs) * key_dim
+    state_mask = (place >= begin) & (place < begin + key_dim)
 
     def gathered(incoming):
         total = incoming[0].astype(F32)
-        for p in range(1, n_kv):
+        for p in range(1, incoming.shape[0]):
             total = total + incoming[p].astype(F32)
         return total
 
@@ -338,25 +384,21 @@
     code = (misc * inv_rms).astype(BF16)
     pre_gate = dot(code, dw[...]) + db[...]
     new_decay = (jnp.minimum(pre_gate, 0.0) - jnp.log1p(jnp.exp(-jnp.abs(pre_gate)))) / GATE_TEMP
-    pairs_here = heads_here * seqs
     decayed = stacked(queries * jnp.exp(new_decay), heads_here)
     own = jnp.sum(
         stacked(queries, heads_here) * stacked(new_keys.astype(F32), heads_here),
         axis=-1,
         keepdims=True,
     )
-
-    def own_block(wide):
-        each = wide.shape[1] // pairs_here
-        pair = lax.broadcasted_iota(jnp.int32, wide.shape, 0)
-        place = lax.broadcasted_iota(jnp.int32, wide.shape, 1)
-        mine = (place >= pair * each) & (place < (pair + 1) * each)
-        return jnp.where(mine, wide, 0.0).astype(BF16)
-
-    into_state = decayed * total_exp[...]
-    carried = dot(own_block(jnp.concatenate([into_state] * pairs_here, axis=1)), state_rows[...])
-    scores = own_block(dot_t(decayed.astype(BF16), keyed_rows[...]))
-    full = carried + dot(scores, value_rows[...])
+    scores = dot_t(decayed.astype(BF16), keyed_rows[...])
+    within = dot(jnp.where(score_mask, scores, 0.0).astype(BF16), value_rows[...])
+    into_state = jnp.concatenate([decayed * total_exp[...]] * pairs_here, axis=1)
+    ready("state")
+    carried = dot(
+        jnp.where(state_mask, into_state, 0.0),
+        state[...].reshape(pairs_here * key_dim, value_dim),
+    )
+    full = carried + within
     drain(proj_recv, recv_sem.at[SEM_PROJ])
     total = gathered(proj_recv)
     new_values = (total[:, :vw] * inv_rms).astype(BF16)
@@ -369,17 +411,17 @@
         heads_send[:, h * value_dim : (h + 1) * value_dim] = mixed[
             h * seqs : (h + 1) * seqs
         ].astype(BF16)
-    to_kv(lambda p: heads_send, heads_all, SEM_HEADS)
+    to_kv(lambda p: heads_send, heads_all, SEM_HEADS, SEM_HEADS + 1)
     values_send[...] = new_values
     send(values_send, values_recv, SEM_VALUES, {"tp": tp_mate})
     pending.append((values_send, SEM_VALUES))
     ready("wo")
     ready("mlp_gain")
-    drain(heads_all, recv_sem.at[SEM_HEADS])
-    for p in range(n_kv):
-        heads[p * seqs : (p + 1) * seqs, :] = heads_all[p].astype(F32)
-    attended[tp_me] = dot(heads[...].astype(BF16), wo[...]).astype(BF16)
-    to_tp(attended, SEM_ATTEND)
+    for block in range(2):
+        await_kv(heads_all, SEM_HEADS + block)
+        part = heads_all[pl.ds(2 * half * block, 2 * half)].reshape(group, vw)
+        attended[block][tp_me] = dot(part, wo[...]).astype(BF16)
+        to_tp(attended[block], SEM_ATTEND + block)
     drain(keys_recv, recv_sem.at[SEM_KEYS])
     drain(values_recv, recv_sem.at[SEM_VALUES])
     for h in range(heads_here):
@@ -390,14 +432,16 @@
             nv_ref[b, h : h + 1, :] = values[b : b + 1].astype(BF16)
     ready("gate")
     ready("up")
-    await_tp(attended, SEM_ATTEND)
-    summed = attended[0].astype(F32)
-    for p in range(1, n_tp):
-        summed = summed + attended[p].astype(F32)
-    mid_f = (token_f + summed).astype(BF16).astype(F32)
-    scaled_mid = (mid_f * mlp_gain[...]).astype(BF16)
-
-    for part, (first, size, span_cols) in enumerate(pieces):
+    mids, mid_squares = [], []
+    for block in range(2):
+        update = summed(attended[block], SEM_ATTEND + block)
+        mid_f = (tokens[rows_of(block), :].astype(F32) + update).astype(BF16).astype(F32)
+        scaled_mid[block * group : (block + 1) * group, :] = (mid_f * mlp_gain[...]).astype(BF16)
+        mids.append(mid_f)
+        mid_squares.append(jnp.sum(mid_f * mid_f, axis=1, keepdims=True))
+
+    for part in COMPUTE:
+        first, size, span_cols = pieces[part]
         mlp_acc = accs[part]
         for base, weight in ((0, gate), (span_cols, up)):
             if size < span_cols:
@@ -406,14 +450,55 @@
                 )
             for start, count in tiles_of(size, 256):
                 mlp_acc[:, base + start : base + start + count] = dot_t(
-                    scaled_mid, weight[first + start : first + start + count, :]
+                    scaled_mid[...], weight[first + start : first + start + count, :]
                 )
         if part == 0:
-            high, low = split_sum(jnp.sum(mid_f * mid_f, axis=1, keepdims=True))
+            high, low = split_sum(jnp.concatenate(mid_squares, axis=0))
             mlp_acc[:, size : size + 1] = high
             mlp_acc[:, size + 1 : size + 2] = low
-        scatter(mlp_acc, sends[part], recvs[part], SHARED_SEMS + part)
-    for part, (first, size, span_cols) in enumerate(pieces):
+        for q in range(n_kv):
+            line = bases[q // (2 * half)] + q % (2 * half) // 2
+            sends[part][q % 2, line] = mlp_acc[q * seqs : (q + 1) * seqs, :].astype(BF16)
+        if part not in PAIRED:
+            to_kv(
+                lambda p, part=part: sends[part].at[lax.rem(p, 2), p // 2],
+                recvs[part],
+                SHARED_SEMS + part,
+                SHARED_SEMS + part,
+            )
+            continue
+        send(
+            sends[part].at[1 - side, pl.ds(far, half)],
+            mate_parts[part],
+            SHARED_SEMS + 2 * PARTS + part,
+            {"kv": kv_me + 1 - 2 * side},
+        )
+        pending.append((mate_parts[part], SHARED_SEMS + 2 * PARTS + part))
+        for k in range(half - 1, -1, -1):
+            line = near + lax.rem(local + k, half)
+            for other in (1 - side, side):
+                send(
+                    sends[part].at[other, line],
+                    recvs[part].at[slots[0]],
+                    SHARED_SEMS + part,
+                    {"kv": line * 2 + other, "tp": tp_mate},
+                )
+        pending.append((recvs[part], SHARED_SEMS + part))
+    for part in PAIRED:
+        drain(mate_parts[part], recv_sem.at[SHARED_SEMS + 2 * PARTS + part])
+        for k in range(half):
+            both = sends[part][side, far + k].astype(F32) + mate_parts[part][k].astype(F32)
+            far_sends[part][k] = both.astype(BF16)
+        for k in range(half):
+            line = lax.rem(local + k, half)
+            send(
+                far_sends[part].at[line],
+                recvs[part].at[2 * half + local],
+                SHARED_SEMS + part,
+                {"kv": (far + line) * 2 + side, "tp": tp_mate},
+            )
+    for part in ORDER:
+        first, size, span_cols = pieces[part]
         drain(recvs[part], recv_sem.at[SHARED_SEMS + part])
         total = gathered(recvs[part])
         if part == 0:
@@ -422,29 +507,39 @@
         g = total[:, :span_cols] * inv_mid
         mine = g / (1.0 + jnp.exp(-g)) * (total[:, span_cols:] * inv_mid)
         hidden_sends[part][...] = mine.astype(BF16)
+        near_sem = SHARED_SEMS + PARTS + part
         to_kv(
-            lambda p, part=part: hidden_sends[part], hiddens_all[part], SHARED_SEMS + PARTS + part
+            lambda p, part=part: hidden_sends[part],
+            hiddens_all[part],
+            near_sem,
+            SEM_TAIL if part == ORDER[-1] else near_sem,
         )
     ready("down")
     acc = jnp.zeros((rows, feats), F32)
-    for part, (first, size, span_cols) in enumerate(pieces):
+
+    def lift(part, blocks):
+        first, size, span_cols = pieces[part]
+        count = len(blocks) * 2 * half
+        hidden = hiddens_all[part][pl.ds(blocks[0] * 2 * half, count)]
+        hidden = hidden.reshape(count * seqs, span_cols)
+        if size < span_cols:
+            lane = lax.broadcasted_iota(jnp.int32, hidden.shape, 1)
+            hidden = jnp.where(lane < size, hidden.astype(F32), 0.0).astype(BF16)
+        return dot(hidden, down[first : first + span_cols, :])
+
+    acc = jnp.zeros((rows, feats), F32)
+    for part in ORDER[:-1]:
         drain(hiddens_all[part], recv_sem.at[SHARED_SEMS + PARTS + part])
-        hidden = hiddens[part]
-        for p in range(n_kv):
-            hidden[p * seqs : (p + 1) * seqs, :] = hiddens_all[part][p].astype(F32)
-        if size < span_cols:
-            lane = lax.broadcasted_iota(jnp.int32, (rows, span_cols), 1)
-            whole = jnp.where(lane < size, hidden[...], 0.0).astype(BF16)
-        else:
-            whole = hidden[...].astype(BF16)
-        acc = acc + dot(whole, down[first : first + span_cols, :])
-    lifted[tp_me] = acc.astype(BF16)
-    to_tp(lifted, SEM_LIFT)
-    await_tp(lifted, SEM_LIFT)
-    summed = lifted[0].astype(F32)
-    for p in range(1, n_tp):
-        summed = summed + lifted[p].astype(F32)
-    out_ref[...] = (mid_f + summed).astype(BF16)
+        acc = acc + lift(part, (0, 1))
+    last = ORDER[-1]
+    for block, sem in enumerate((SHARED_SEMS + PARTS + last, SEM_TAIL)):
+        await_kv(hiddens_all[last], sem)
+        ending = acc[block * group : (block + 1) * group] + lift(last, (block,))
+        lifted[block][tp_me] = ending.astype(BF16)
+        to_tp(lifted[block], SEM_LIFT + block)
+    for block in range(2):
+        update = summed(lifted[block], SEM_LIFT + block)
+        out_ref[rows_of(block), :] = (mids[block] + update).astype(BF16)
     for load in given:
         load.wait_send()
     for ref, sem in pending:
@@ -475,6 +570,7 @@
         down,
     ) = args
     row = lambda a: a.reshape(1, a.shape[0])
+    by_position = lambda a: a.reshape(a.shape[0], a.shape[1] * a.shape[2], a.shape[3])
     operands = [
         tokens,
         row(attn_gain),
@@ -486,9 +582,9 @@
         dw,
         row(db),
         row(head_gain),
-        key,
+        by_position(key),
         value,
-        decay,
+        by_position(decay),
         state,
         lengths,
         wo,
@@ -517,40 +613,39 @@
 
     scratch = [copied(a) for a in operands]
     scratch += [
+        vmem((rows, feats), BF16),
         vmem((rows, first_cols), F32),
         vmem((n_kv, seqs, first_cols), BF16),
         vmem((n_kv, seqs, first_cols), BF16),
         vmem((rows, cols), F32),
         vmem((n_kv, seqs, cols), BF16),
         vmem((n_kv, seqs, cols), BF16),
-        vmem((seqs, span, heads_here, key_dim), F32),
         vmem((pairs * span, key_dim), BF16),
         vmem((pairs * span, value_dim), BF16),
-        vmem((pairs * key_dim, value_dim), BF16),
         vmem((pairs, key_dim), F32),
         vmem((seqs, kw), BF16),
         vmem((seqs, kw), BF16),
         vmem((seqs, vw), BF16),
         vmem((seqs, vw), BF16),
         vmem((seqs, vw), BF16),
-        vmem((rows, vw), F32),
         vmem((n_kv, seqs, vw), BF16),
-        vmem((n_tp, rows, feats), BF16),
+        [vmem((n_tp, rows // 2, feats), BF16)] * 2,
         [vmem((rows, 2 * w), F32) for w in widths],
-        [vmem((n_kv, seqs, 2 * w), BF16) for w in widths],
-        [vmem((n_kv, seqs, 2 * w), BF16) for w in widths],
-        [vmem((rows, w), F32) for w in widths],
+        [vmem((2, n_kv // 2, seqs, 2 * w), BF16) for w in widths],
+        [vmem((slots, seqs, 2 * w), BF16) for slots, w in zip(slots_of(n_kv), widths)],
+        [vmem((n_kv // 4, seqs, 2 * w), BF16) for w in widths],
+        [vmem((n_kv // 4, seqs, 2 * w), BF16) for w in widths],
         [vmem((seqs, w), BF16) for w in widths],
         [vmem((n_kv, seqs, w), BF16) for w in widths],
-        vmem((n_tp, rows, feats), BF16),
+        [vmem((n_tp, rows // 2, feats), BF16)] * 2,
     ]
     dma = pltpu.SemaphoreType.DMA
     scratch += [dma((len(operands) + len(SWAPPED_LOADS),))]
-    scratch += [dma((SHARED_SEMS + 2 * PARTS,))] * 2
+    scratch += [dma((SHARED_SEMS + 3 * PARTS,))] * 2
     in_specs = [pl.BlockSpec(memory_space=pltpu.HBM)] * len(operands)
     shapes = ((rows, feats), (seqs, heads_here, key_dim), (seqs, heads_here, value_dim))
     results = pl.pallas_call(
-        functools.partial(layer_kernel, n_kv, n_tp, feats * n_kv),
+        functools.partial(layer_kernel, n_kv, n_tp, feats * n_kv, heads_here),
         out_shape=tuple(vmem(shape, BF16) for shape in shapes),
         in_specs=in_specs,
         out_specs=(pl.BlockSpec(memory_space=pltpu.VMEM),) * 3,

time: 38.3 us -> 35.5 us (0.927)
  Pallas kernels: 37.5 us -> 34.7 us
    pallas_call x1, Pallas kernels: 36.8 us -> 34 us  [on_device(): pl.pallas_call(functools.partial(layer_kernel, n_kv, n_tp, feats * n_kv,...]
where the time goes in v3:
time: 35.5 us; the launch traced here: 35.3 us
  Pallas kernels  34.7 us (98%)
  between operations  0.65 us (2%)
    pallas_call x1, Pallas kernels, on_device(): pl.pallas_call(functools.partial(layer_kernel, n_kv, n_tp, feats * n_kv,...  34 us

profile of v3, /device:TPU:0, one launch (start us, length us, event | category | flops | bytes accessed | tf_op | source)
XLA Modules:
  0.0 35.3 jit_solution(13628749160250672604)
XLA Ops:
  0.6 34.0 %layer.1 = (bf16[32,512]{1,0:T(8,128)(2,1)S(1)}, bf16[4,2,128]{2,1,0:T(2,128)(2,1)S(1)}, bf16[4,2,256]{2,1,0:T(2,128)(2,1)S(1)}) custom-call(bf16[32,512]{1,0:T(8,128)(2,1)} %tokens_h.1, f32[1,512]{1,0:T(1,128)} %bitcast.14, bf16[512,256]{1,0:T(8,128)(2,1)} %wq_h.1, bf16[512,256]{1,0:T(8,128)(2,1)} %wk_h.1, bf16[512,512]{1,0:T(8,128)(2,1)} %wv_h.1, ...), custom_call_target="tpu_custom_call" | custom-call | tf_op jit(solution)/shard_map/layer/pallas_call | solution.py:647
  34.7 0.6 %results.1 = (bf16[32,512]{1,0:T(8,128)(2,1)}, bf16[4,2,128]{2,1,0:T(2,128)(2,1)}, bf16[4,2,256]{2,1,0:T(2,128)(2,1)}) custom-call(bf16[32,512]{1,0:T(8,128)(2,1)S(1)} %get-tuple-element.6.refs_0_, bf16[4,2,128]{2,1,0:T(2,128)(2,1)S(1)} %get-tuple-element.7.refs_1_, bf16[4,2,256]{2,1,0:T(2,128)(2,1)S(1)} %get-tuple-element.8.refs_2_), custom_call_target="tpu_custom_call" | custom-call | tf_op jit(solution)/shard_map/results/pallas_call | solution.py:658
